TPU v7x, 32 devices: a whole 2x2x4 slice. The times are simulated.
32 devices in a mesh: sp: 4 (over z), fs: 4 (over y, x), tp: 2 (over core).
Axes of the slice: x: 2, y: 2, z: 4, core: 2. Of those that a mesh axis runs over, the one named last changes fastest.
Arguments:
- output_gate_logits: bfloat16 [4, 512, 2048], P('fs', 'sp', 'tp'), may hold values from -6 to 6
- head_input_rows: bfloat16 [4, 512, 2048], P('fs', 'sp', 'tp'), may hold values from -6 to 6
- group_state_writes: bfloat16 [4, 512, 512], P('fs', 'sp', 'tp'), may hold values from -6 to 6
- group_state_reads: bfloat16 [4, 512, 512], P('fs', 'sp', 'tp'), may hold values from -6 to 6
- step_logits: float32 [4, 512, 32], P('fs', 'sp', 'tp'), may hold values from -5 to 5
- head_step_offset: float32 [32], P('tp'), may hold values from -3.5 to 1
- head_decay_logrates: float32 [32], P('tp'), may hold values from -11 to 0
- decay_extra_spikes: float32 [512, 32], P('sp', 'tp'), may hold values from -2.1 to 0
- head_input_taps: bfloat16 [4, 2048], P(None, 'tp'), may hold values from -3 to 3
- state_input_taps: bfloat16 [4, 512], P(None, 'tp'), may hold values from -3 to 3
- readout_filter_taps: bfloat16 [4, 512], P(None, 'tp'), may hold values from -3 to 3
- grouped_norm_scale: float32 [2048], P('tp'), may hold values from 0.1 to 1.9
- convolution_outer_gate: bfloat16 [4, 512, 1024], P('fs', 'sp', 'tp'), may hold values from -6 to 6
- convolution_inner_gate: bfloat16 [4, 512, 1024], P('fs', 'sp', 'tp'), may hold values from -6 to 6
- convolution_value_rows: bfloat16 [4, 512, 1024], P('fs', 'sp', 'tp'), may hold values from -6 to 6
- gated_filter_taps: bfloat16 [3, 1024], P(None, 'tp'), may hold values from -3.5 to 3.5
- state_output_rows: bfloat16 [2048, 2048], P('tp', 'fs'), may hold values from -0.09375 to 0.09375
- convolution_output_rows: bfloat16 [1024, 2048], P('tp', 'fs'), may hold values from -0.125 to 0.125
Outputs:
- layer_out: bfloat16 [4, 512, 2048], P('tp', 'sp', 'fs')
All inputs are finite; a program needn't handle non-finite values.
Results may differ from a plain program's by a relative error of at most 0.012.
Values may be sent and summed in bfloat16 or wider, within the bound.
A program may use at most 64 MiB of HBM per device.

v0:
```python
import jax
import jax.numpy as jnp
from jax import lax
from jax.sharding import PartitionSpec as P

STATE = 128
BLOCK = 128


EPS = 1e-06
HIGH = lax.Precision.HIGHEST


def shifted(value, axis, steps):
    count = lax.axis_size(axis)
    first, last = (max(0, -steps), min(count, count - steps))
    return lax.ppermute(value, axis, [(source, source + steps) for source in range(first, last)])


def entering(array, axis, combine, identity):
    size, place = (lax.axis_size(axis), lax.axis_index(axis))
    everything = jax.tree.map(
        lambda part, kind: lax.all_gather(part.astype(kind), axis),
        array,
        (jnp.bfloat16, jnp.bfloat16),
    )
    start = jax.tree.map(
        lambda part, zero: jnp.broadcast_to(jnp.asarray(zero, part.dtype), part.shape),
        array,
        identity,
    )

    def turn(k, before):
        reached = k < place
        new = combine(
            before, jax.tree.map(lambda part, own: part[k].astype(own.dtype), everything, array)
        )
        return jax.tree.map(lambda a, b: jnp.where(reached, a, b), new, before)

    return lax.fori_loop(0, size, turn, start)


def causal_filter(stream, kernel, before):
    span = kernel.shape[0]
    length = stream.shape[1]
    padded = jnp.concatenate([before, stream], axis=1)
    total = padded[:, 0:length] * kernel[0]
    for offset in range(1, span):
        total = total + padded[:, offset : offset + length] * kernel[offset]
    return total


def block_scan(driven, decay, writes, reads):
    batch, length, groups, ratio, channels = driven.shape
    entries = writes.shape[-1]
    count = length // BLOCK

    def split(array):
        shaped = array.reshape((batch, count, BLOCK) + array.shape[2:])
        return jnp.moveaxis(shaped, 1, 0)

    causal = jnp.tril(jnp.ones((BLOCK, BLOCK), dtype=bool))

    def advance(carry, pieces):
        drive, fall, write, read = pieces
        rising = jnp.cumsum(fall, axis=1)
        scores = jnp.einsum("blgn,bsgn->bgls", read, write, precision=HIGH)
        gaps = rising[:, :, None] - rising[:, None, :]
        weights = jnp.exp(jnp.where(causal[None, :, :, None, None], gaps, -jnp.inf))
        inside = jnp.einsum("bgls,blsgr,bsgrp->blgrp", scores, weights, drive, precision=HIGH)
        earlier = (
            jnp.einsum("blgn,bgrpn->blgrp", read, carry, precision=HIGH)
            * jnp.exp(rising)[..., None]
        )
        remain = jnp.exp(rising[:, -1:] - rising)
        fresh = jnp.einsum("bsgn,bsgr,bsgrp->bgrpn", write, remain, drive, precision=HIGH)
        carry = carry * jnp.exp(rising[:, -1])[..., None, None] + fresh
        return (carry, inside + earlier)

    start = jnp.zeros((batch, groups, ratio, channels, entries), jnp.float32)
    final, blocks = lax.scan(
        advance, start, (split(driven), split(decay), split(writes), split(reads))
    )
    return (final, jnp.moveaxis(blocks, 0, 1).reshape(driven.shape))


def join_states(earlier, later):
    total_early, state_early = earlier
    total_late, state_late = later
    return (
        total_early + total_late,
        state_early * jnp.exp(total_late)[..., None, None] + state_late,
    )


def per_device(
    output_gate_logits,
    head_input_rows,
    group_state_writes,
    group_state_reads,
    step_logits,
    head_step_offset,
    head_decay_logrates,
    decay_extra_spikes,
    head_input_taps,
    state_input_taps,
    readout_filter_taps,
    grouped_norm_scale,
    convolution_outer_gate,
    convolution_inner_gate,
    convolution_value_rows,
    gated_filter_taps,
    state_output_rows,
    convolution_output_rows,
):
    batch, length, head_width = head_input_rows.shape
    heads = step_logits.shape[2]
    group_width = group_state_writes.shape[2]
    groups = group_width // STATE
    ratio = heads // groups
    channels = head_width // heads
    conv_width = convolution_inner_gate.shape[2]
    reach = head_input_taps.shape[0] - 1
    short = gated_filter_taps.shape[0] - 1
    rims = jnp.concatenate(
        [
            head_input_rows[:, -reach:],
            group_state_writes[:, -reach:],
            group_state_reads[:, -reach:],
            convolution_inner_gate[:, -reach:],
            convolution_value_rows[:, -reach:],
        ],
        axis=2,
    )
    before = shifted(rims, "sp", 1).astype(jnp.float32)
    second = head_width + group_width
    third = second + group_width
    fourth = third + conv_width
    before_input = before[:, :, :head_width]
    before_writes = before[:, :, head_width:second]
    before_reads = before[:, :, second:third]
    before_inner = before[:, reach - short :, third:fourth]
    before_values = before[:, reach - short :, fourth:]
    product = convolution_inner_gate.astype(jnp.float32) * convolution_value_rows.astype(
        jnp.float32
    )
    filtered = causal_filter(
        product, gated_filter_taps.astype(jnp.float32), before_inner * before_values
    )
    conv_branch = (convolution_outer_gate.astype(jnp.float32) * filtered).astype(jnp.bfloat16)
    conv_rows = conv_branch.reshape(batch * length, conv_width)
    filtered_input = jax.nn.silu(
        causal_filter(
            head_input_rows.astype(jnp.float32), head_input_taps.astype(jnp.float32), before_input
        )
    )
    filtered_writes = jax.nn.silu(
        causal_filter(
            group_state_writes.astype(jnp.float32),
            state_input_taps.astype(jnp.float32),
            before_writes,
        )
    )
    filtered_reads = jax.nn.silu(
        causal_filter(
            group_state_reads.astype(jnp.float32),
            readout_filter_taps.astype(jnp.float32),
            before_reads,
        )
    )
    head_step_length = jax.nn.softplus(step_logits + head_step_offset)
    decay_logarithm = decay_extra_spikes[None] - head_step_length * jnp.exp(head_decay_logrates)
    driven = (
        filtered_input.reshape(batch, length, heads, channels) * head_step_length[..., None]
    ).reshape(batch, length, groups, ratio, channels)
    decay_grouped = decay_logarithm.reshape(batch, length, groups, ratio)
    reads_grouped = filtered_reads.reshape(batch, length, groups, STATE)
    final, inside = block_scan(
        driven, decay_grouped, filtered_writes.reshape(batch, length, groups, STATE), reads_grouped
    )
    totals = jnp.sum(decay_grouped, axis=1)
    prefix = entering(
        (totals, final), "sp", join_states, (jnp.zeros_like(totals), jnp.zeros_like(final))
    )
    incoming = prefix[1]
    rising = jnp.cumsum(decay_grouped, axis=1)
    carried = (
        jnp.einsum("blgn,bgrpn->blgrp", reads_grouped, incoming, precision=HIGH)
        * jnp.exp(rising)[..., None]
    )
    state_output = (inside + carried).reshape(batch, length, head_width)
    gated = state_output * jax.nn.silu(output_gate_logits.astype(jnp.float32))
    grouped = gated.reshape(batch, length, groups, ratio * channels)
    normed = grouped * lax.rsqrt(jnp.mean(grouped * grouped, axis=-1, keepdims=True) + EPS)
    state_branch = (normed.reshape(batch, length, head_width) * grouped_norm_scale).astype(
        jnp.bfloat16
    )
    state_rows = state_branch.reshape(batch * length, head_width)
    conv_terms = jnp.dot(
        lax.all_gather(conv_rows, "fs", axis=0, tiled=True),
        convolution_output_rows,
        preferred_element_type=jnp.float32,
    )
    conv_sum = lax.psum_scatter(
        conv_terms.astype(jnp.bfloat16), "tp", scatter_dimension=0, tiled=True
    ).astype(jnp.float32)
    state_terms = jnp.dot(
        lax.all_gather(state_rows, "fs", axis=0, tiled=True),
        state_output_rows,
        preferred_element_type=jnp.float32,
    )
    state_sum = lax.psum_scatter(
        state_terms.astype(jnp.bfloat16), "tp", scatter_dimension=0, tiled=True
    ).astype(jnp.float32)
    summed = state_sum + conv_sum
    return summed.astype(jnp.bfloat16).reshape(-1, length, summed.shape[1])


def solution(mesh):
    return jax.shard_map(
        per_device,
        mesh=mesh,
        in_specs=(
            P("fs", "sp", "tp"),
            P("fs", "sp", "tp"),
            P("fs", "sp", "tp"),
            P("fs", "sp", "tp"),
            P("fs", "sp", "tp"),
            P("tp"),
            P("tp"),
            P("sp", "tp"),
            P(None, "tp"),
            P(None, "tp"),
            P(None, "tp"),
            P("tp"),
            P("fs", "sp", "tp"),
            P("fs", "sp", "tp"),
            P("fs", "sp", "tp"),
            P(None, "tp"),
            P("tp", "fs"),
            P("tp", "fs"),
        ),
        out_specs=P("tp", "sp", "fs"),
        check_vma=False,
    )
```

profile of v0, /device:TPU:25, one launch (start us, length us, event | category | flops | bytes accessed | tf_op | source)
XLA Modules:
  0.0 106.1 jit_solution(11196105492878166526)
XLA Ops:
  7.4 0.8 constant_dynamic-update-slice_fusion.4
  9.6 0.7 constant_dynamic-update-slice_fusion.1
  10.3 0.7 constant_dynamic-update-slice_fusion
  11.0 1.4 %collective-permute-start = (bf16[1,3,2560]{2,1,0:T(4,128)(2,1)S(1)}, bf16[1,3,2560]{2,1,0:T(4,128)(2,1)S(1)}, u32[]{:S(2)}, u32[]{:S(2)}) collective-permute-start(bf16[1,3,2560]{2,1,0:T(4,128)(2,1)S(1)} %constant_dynamic-update-slice_fusion), channel_id=1, source_target_pairs={{0,8},{8,16},{16,24},{1,9},{9,17},{17,25},{2,10},{10,18},{18,26},{... | collective-permute-start | bytes 46088 | tf_op jit(solution)/shard_map/ppermute | solution.py:17
  16.3 1.4 %divide_multiply_fusion = f32[1,128,1024]{1,2,0:T(8,128)S(1)} fusion(f32[1,128,1024]{1,2,0:T(8,128)S(1)} %convert_element_type.115, f32[1,3,1024]{1,2,0:T(8,128)S(1)} %copy.60, f32[1024]{0:T(1024)S(1)} %bitcast.107, f32[1024]{0:T(1024)S(1)} %bitcast.106, f32[1024]{0:T(1024)S(1)} %bitcast.105, f32[1024]{0:T(1024)S(1)} %bitcast.104), kind=kLoop, calls=%fused_computation.46 | loop fusion | flops 1835008 | bytes 1077248 | tf_op jit(solution)/shard_map/jit(silu)/mul | solution.py:152
  17.7 1.3 %fusion.5 = bf16[2,8,64,128]{3,2,1,0:T(8,128)(2,1)} fusion(f32[128,2,8,64]{0,3,2,1:T(8,128)S(1)} %bitcast.94, f32[128,2,8]{0,2,1:T(8,128)S(1)} %copy.63, f32[2,8]{1,0:T(2,128)S(1)} %exponential_multiply_fusion, f32[128,2,8]{0,2,1:T(8,128)S(1)} %get-tuple-element.173, f32[128,2,128,1]{2,1,0,3:T(2,128)S(1)} %bitcast.101), kind=kOutput, calls=%fused_computation.17 | convolution fusion | flops 201850880 | bytes 933952 | tf_op jit(solution)/shard_map/while/body/eval_jaxpr/bsgn,bsgr,bsgrp->bgrpn/dot_general | solution.py:76
  19.2 6.1 %all_gather.16 = bf16[4,1,2,8]{3,2,1,0:T(2,128)(2,1)S(1)} all-gather(bf16[1,1,2,8]{3,2,1,0:T(2,128)(2,1)S(1)} %convert_element_type.118), channel_id=1, replica_groups=mesh['sp'=4,'fs'=4,'tp'=2] {'sp'}, dimensions={0}, use_global_device_ids=true | all-gather | bytes 160 | tf_op jit(solution)/shard_map/all_gather | solution.py:23
  25.9 0.7 copy-done.3
  27.9 19.8 %all-gather.6.cloned.1.call-done = bf16[8,8,64,128]{3,2,1,0:T(8,128)(2,1)} async-done(((bf16[2,8,64,128]{3,2,1,0:T(8,128)(2,1)}), bf16[8,8,64,128]{3,2,1,0:T(8,128)(2,1)}) %all-gather.6.cloned.1.call-update) | async-done | bytes 1048592 | tf_op jit(solution)/shard_map/all_gather | solution.py:23
  47.7 4.5 %while.9 = (s32[]{:T(128)}, f32[1,2,8,64,128]{4,3,2,1,0:T(8,128)S(1)}, s32[]{:T(128)}, bf16[4,1,2,8]{3,2,1,0:T(2,128)(2,1)S(1)}, bf16[4,1,2,8,64,128]{5,4,3,2,1,0:T(8,128)(2,1)}, /*index=5*/s32[]{:T(128)}, s32[]{:T(128)}) while((s32[]{:T(128)}, f32[1,2,8,64,128]{4,3,2,1,0:T(8,128)S(1)}, s32[]{:T(128)}, ...), condition=%wide.region_3.4_spmd.clone, body=%wide.region_2.3_spmd.clone.sunk | while | flops 655380 | bytes 1310985 | solution.py:40
  47.7 1.1 %fusion.84 = f32[1,2,8,64,128]{4,3,2,1,0:T(8,128)S(1)} fusion(f32[1,2,8,64,128]{4,3,2,1,0:T(8,128)S(1)} %get-tuple-element.230, bf16[4,1,2,8,64,128]{5,4,3,2,1,0:T(8,128)(2,1)} %get-tuple-element.240, s32[]{:T(128)} %get-tuple-element.229, f32[2,8]{1,0:T(2,128)S(1)} %exponential_bitcast_fusion.2, pred[]{:T(512)S(6)} %compare.3, pred[]{:T(512)S(6)} %lt.23), kind=kLoop, calls=%fused_computation.1.clone.1 | loop fusion | flops 655360 | bytes 1310790 | tf_op jit(solution)/shard_map/while/body/eval_jaxpr/jit(_where)/select_n | solution.py:38
  48.8 1.1 %fusion.84 = f32[1,2,8,64,128]{4,3,2,1,0:T(8,128)S(1)} fusion(f32[1,2,8,64,128]{4,3,2,1,0:T(8,128)S(1)} %get-tuple-element.230, bf16[4,1,2,8,64,128]{5,4,3,2,1,0:T(8,128)(2,1)} %get-tuple-element.240, s32[]{:T(128)} %get-tuple-element.229, f32[2,8]{1,0:T(2,128)S(1)} %exponential_bitcast_fusion.2, pred[]{:T(512)S(6)} %compare.3, pred[]{:T(512)S(6)} %lt.23), kind=kLoop, calls=%fused_computation.1.clone.1 | loop fusion | flops 655360 | bytes 1310790 | tf_op jit(solution)/shard_map/while/body/eval_jaxpr/jit(_where)/select_n | solution.py:38
  50.0 1.1 %fusion.84 = f32[1,2,8,64,128]{4,3,2,1,0:T(8,128)S(1)} fusion(f32[1,2,8,64,128]{4,3,2,1,0:T(8,128)S(1)} %get-tuple-element.230, bf16[4,1,2,8,64,128]{5,4,3,2,1,0:T(8,128)(2,1)} %get-tuple-element.240, s32[]{:T(128)} %get-tuple-element.229, f32[2,8]{1,0:T(2,128)S(1)} %exponential_bitcast_fusion.2, pred[]{:T(512)S(6)} %compare.3, pred[]{:T(512)S(6)} %lt.23), kind=kLoop, calls=%fused_computation.1.clone.1 | loop fusion | flops 655360 | bytes 1310790 | tf_op jit(solution)/shard_map/while/body/eval_jaxpr/jit(_where)/select_n | solution.py:38
  51.1 1.1 %fusion.84 = f32[1,2,8,64,128]{4,3,2,1,0:T(8,128)S(1)} fusion(f32[1,2,8,64,128]{4,3,2,1,0:T(8,128)S(1)} %get-tuple-element.230, bf16[4,1,2,8,64,128]{5,4,3,2,1,0:T(8,128)(2,1)} %get-tuple-element.240, s32[]{:T(128)} %get-tuple-element.229, f32[2,8]{1,0:T(2,128)S(1)} %exponential_bitcast_fusion.2, pred[]{:T(512)S(6)} %compare.3, pred[]{:T(512)S(6)} %lt.23), kind=kLoop, calls=%fused_computation.1.clone.1 | loop fusion | flops 655360 | bytes 1310790 | tf_op jit(solution)/shard_map/while/body/eval_jaxpr/jit(_where)/select_n | solution.py:38
  52.8 2.3 %fusion.2 = f32[1,128,2,8,64]{1,4,3,2,0:T(8,128)S(1)} fusion(f32[1,128,2,8,64]{1,4,3,2,0:T(8,128)S(1)} %fusion.4, f32[1,128,2,8,64]{1,4,3,2,0:T(8,128)S(1)} %fusion.3, f32[128,2,8]{0,2,1:T(8,128)S(1)} %copy.57, f32[128,128,2]{1,0,2:T(8,128)S(1)} %convolution_bitcast_fusion.3, pred[128,128]{1,0:T(8,128)(4,1)S(1)} %iota_compare_fusion, ...), kind=kOutput, calls=%fused_computation.14 | convolution fusion | flops 202506240 | bytes 2260992 | tf_op jit(solution)/shard_map/while/body/eval_jaxpr/bgls,blsgr,bsgrp->blgrp/dot_general | solution.py:70
  56.0 0.9 fusion.25
  57.0 0.8 copy-done.4
  57.9 0.8 copy-done.6
  58.9 8.3 %all-gather.2 = bf16[1,512,512]{2,1,0:T(8,128)(2,1)S(1)} all-gather(bf16[1,128,512]{2,1,0:T(8,128)(2,1)S(1)} %fusion.40), channel_id=4, replica_groups=mesh['sp'=4,'fs'=4,'tp'=2] {'fs'}, dimensions={1}, use_global_device_ids=true | all-gather | bytes 655360 | tf_op jit(solution)/shard_map/all_gather | solution.py:200
  67.2 1.2 %convolution_convert_fusion = bf16[512,512]{1,0:T(8,128)(2,1)} fusion(bf16[512,512]{1,0:T(8,128)(2,1)S(1)} %copy-done.1, bf16[1,512,512]{2,1,0:T(8,128)(2,1)S(1)} %all-gather.2), kind=kOutput, calls=%fused_computation.3 | convolution fusion | flops 268697600 | bytes 1572864 | tf_op jit(solution)/shard_map/dot_general | solution.py:199
  68.5 16.7 %all-gather.8.cloned.1.call-done = bf16[1,512,1024]{1,2,0:T(8,128)(2,1)} async-done(((bf16[1,128,1024]{1,2,0:T(8,128)(2,1)}), bf16[1,512,1024]{1,2,0:T(8,128)(2,1)}) %all-gather.8.cloned.1.call-update) | async-done | bytes 1048592 | tf_op jit(solution)/shard_map/all_gather | solution.py:208
  85.2 2.8 %convolution_convert_fusion.1 = bf16[512,512]{1,0:T(8,128)(2,1)} fusion(bf16[1024,512]{1,0:T(8,128)(2,1)S(1)} %copy-done, bf16[1,512,1024]{1,2,0:T(8,128)(2,1)} %all-gather.8.cloned.1.call-done), kind=kOutput, calls=%fused_computation.4 | convolution fusion | flops 537133056 | bytes 2621440 | tf_op jit(solution)/shard_map/dot_general | solution.py:207
  88.0 8.9 %reduce-scatter.3.cloned.1.call-done = bf16[256,512]{1,0:T(8,128)(2,1)} async-done(((bf16[512,512]{1,0:T(8,128)(2,1)}), bf16[256,512]{1,0:T(8,128)(2,1)}) %reduce-scatter.3.cloned.1.call-update) | async-done | bytes 262160 | tf_op jit(solution)/shard_map/reduce_scatter | solution.py:212
  96.9 1.8 %add_convert_fusion = bf16[256,512]{1,0:T(8,128)(2,1)} fusion(bf16[256,512]{1,0:T(8,128)(2,1)} %reduce-scatter.5.cloned.1.call-done, bf16[256,512]{1,0:T(8,128)(2,1)} %reduce-scatter.3.cloned.1.call-done), kind=kLoop, calls=%fused_computation.44 | loop fusion | flops 524288 | bytes 786432 | tf_op jit(solution)/shard_map/convert_element_type | solution.py:216
  (91 shorter events, 8.8 us)
Async XLA Ops:
  7.4 77.8 %copy-start = (bf16[1024,512]{1,0:T(8,128)(2,1)S(1)}, bf16[1024,512]{1,0:T(8,128)(2,1)}, u32[]{:S(2)}) copy-start(bf16[1024,512]{1,0:T(8,128)(2,1)} %param.36) | copy-start | bytes 3145732
  7.4 40.3 %all-gather.6.cloned.1.call-start = ((), (), s32[]{:S(2)}) async-start(), calls=%async_computation.4 | async-start | bytes 1310720 | tf_op jit(solution)/shard_map/all_gather | solution.py:23
  10.3 2.2 %copy-start.11 = (bf16[4,256]{1,0:T(4,128)(2,1)S(1)}, bf16[4,256]{1,0:T(4,128)(2,1)}, u32[]{:S(2)}) copy-start(bf16[4,256]{1,0:T(4,128)(2,1)} %param.30) | copy-start | bytes 6148
  10.3 2.2 %copy-start.12 = (bf16[4,256]{1,0:T(4,128)(2,1)S(1)}, bf16[4,256]{1,0:T(4,128)(2,1)}, u32[]{:S(2)}) copy-start(bf16[4,256]{1,0:T(4,128)(2,1)} %param.29) | copy-start | bytes 6148
  11.0 1.5 %copy-start.9 = (bf16[4,1024]{1,0:T(4,128)(2,1)S(1)}, bf16[4,1024]{1,0:T(4,128)(2,1)}, u32[]{:S(2)}) copy-start(bf16[4,1024]{1,0:T(4,128)(2,1)} %param.28) | copy-start | bytes 24580
  11.0 4.7 %collective-permute-start = (bf16[1,3,2560]{2,1,0:T(4,128)(2,1)S(1)}, bf16[1,3,2560]{2,1,0:T(4,128)(2,1)S(1)}, u32[]{:S(2)}, u32[]{:S(2)}) collective-permute-start(bf16[1,3,2560]{2,1,0:T(4,128)(2,1)S(1)} %constant_dynamic-update-slice_fusion), channel_id=1, source_target_pairs={{0,8},{8,16},{16,24},{1,9},{9,17},{17,25},{2,10},{10,18},{18,26},{... | collective-permute-start | bytes 46088 | tf_op jit(solution)/shard_map/ppermute | solution.py:17
  12.5 0.7 copy-start.17
  12.5 0.7 copy-start.13
  12.5 0.7 copy-start.14
  13.2 0.7 copy-start.16
  14.3 0.8 copy-start.7
  14.3 0.9 copy-start.8
  14.5 1.0 copy-start.2
  19.1 66.1 %all-gather.8.cloned.1.call-start = ((), (), s32[]{:S(2)}) async-start(), calls=%async_computation.5 | async-start | bytes 1310720 | tf_op jit(solution)/shard_map/all_gather | solution.py:208
  25.7 1.0 copy-start.3
  55.3 0.7 copy-start.15
  56.0 1.0 copy-start.10
  56.9 0.9 copy-start.4
  56.9 1.0 copy-start.5
  56.9 31.1 %reduce-scatter.5.cloned.1.call-start = ((), (), s32[]{:S(2)}) async-start(), calls=%async_computation.3 | async-start | bytes 786432 | tf_op jit(solution)/shard_map/reduce_scatter | solution.py:204
  57.8 0.9 copy-start.6
  58.8 8.4 %copy-start.1 = (bf16[512,512]{1,0:T(8,128)(2,1)S(1)}, bf16[512,512]{1,0:T(8,128)(2,1)}, u32[]{:S(2)}) copy-start(bf16[512,512]{1,0:T(8,128)(2,1)} %param.37) | copy-start | bytes 1572868
  68.5 28.5 %reduce-scatter.3.cloned.1.call-start = ((), (), s32[]{:S(2)}) async-start(), calls=%async_computation.2 | async-start | bytes 786432 | tf_op jit(solution)/shard_map/reduce_scatter | solution.py:212
Sparse Core Ops, SparseCore 0:
  19.2 28.4 all-gather.5
  57.0 28.1 all-gather.7
Sparse Core Ops, SparseCore 1:
  68.5 13.0 reduce-scatter.4
  88.1 8.8 reduce-scatter.2
where the time goes:
time: 108 us; the launch traced here: 106 us
  waiting for transfers between devices  45.5 us (42%)
  between operations  15.2 us (14%)
  blocking collectives  14.4 us (13%)
  local copies, waits for them, and re-layouts  10.3 us (10%)
  other arithmetic  9.86 us (9%)
  matrix products  9.16 us (8%)
  starting transfers between devices  1.54 us (1%)
    all_gather x1, waiting for transfers between devices, entering(): lax.all_gather(part.astype(kind), axis)  19.8 us
    all_gather x1, waiting for transfers between devices, per_device(): lax.all_gather(state_rows, 'fs', axis=0, tiled=True)  16.7 us
    reduce_scatter x1, waiting for transfers between devices, per_device(): lax.psum_scatter(state_terms.astype(jnp.bfloat16), 'tp', scatter_dimensio...  8.88 us
    unnamed x42, local copies, waits for them, and re-layouts  8.48 us
    all_gather x1, blocking collectives, per_device(): lax.all_gather(conv_rows, 'fs', axis=0, tiled=True)  8.33 us
    all_gather x1, blocking collectives, entering(): lax.all_gather(part.astype(kind), axis)  6.09 us
    select_n x4, other arithmetic, turn(): return jax.tree.map(lambda a, b: jnp.where(reached, a, b), new, before)  4.4 us
    dot_general x1, matrix products, per_device(): jnp.dot(lax.all_gather(state_rows, 'fs', axis=0, tiled=True), state_outpu...  2.77 us
  transfers between devices with their start and end apart: 5, of which 3 were waited for; matrix products, arithmetic and copies ran while one was open for 7% of the time, Pallas kernels for 0%

commit v1 on v0

v1 whole, which is shorter than its diff:
```python
import functools

import jax
import jax.numpy as jnp
from jax import lax
from jax.experimental import pallas as pl
from jax.experimental.pallas import tpu as pltpu
from jax.sharding import PartitionSpec as P

STATE = 128
EPS = 1e-06
LANES = 128
HALO = 8
HIGH = lax.Precision.HIGHEST
MESH = pl.DeviceIdType.MESH
F32 = jnp.float32
BF16 = jnp.bfloat16


def mm(a, b):
    return jnp.dot(a, b, preferred_element_type=F32)


def silu(v):
    return v / (1.0 + jnp.exp(-v))


def kernel(
    sizes,
    gate_ref,
    head_ref,
    writes_ref,
    reads_ref,
    step_ref,
    offset_ref,
    rate_ref,
    spike_ref,
    head_taps,
    write_taps,
    read_taps,
    scale_ref,
    outer_ref,
    inner_ref,
    value_ref,
    conv_taps,
    wstate_hbm,
    wconv_hbm,
    out_ref,
    head_halo,
    write_halo,
    read_halo,
    inner_halo,
    value_halo,
    head_pad,
    group_pad,
    conv_pad,
    local_state,
    state_send,
    state_recv,
    inside,
    branch_send,
    branch_recv,
    conv_send,
    conv_recv,
    wstate,
    wconv,
    acc,
    halo_ss,
    halo_rs,
    state_ss,
    state_rs,
    branch_ss,
    branch_rs,
    conv_ss,
    conv_rs,
    weight_ss,
    weight_rs,
    local_sem,
):
    nsp, nfs, ntp = sizes
    sp, fs, tp = lax.axis_index("sp"), lax.axis_index("fs"), lax.axis_index("tp")
    length, width = head_ref.shape[1:]
    heads = step_ref.shape[2]
    channels = width // heads
    group_width = writes_ref.shape[2]
    groups = group_width // STATE
    ratio = heads // groups
    gw = ratio * channels
    per_tp = nfs // ntp
    chunks = width // LANES
    per_group = chunks // groups
    hpl = LANES // channels
    dest = fs // per_tp
    slot = lax.rem(fs, per_tp)
    first, last = sp == 0, sp == nsp - 1

    def at(s, f, t):
        return (s, f, t)

    barrier = pltpu.get_barrier_semaphore()
    for a in range(nfs):
        for b in range(ntp):
            if a == 0 and b == 0:
                continue
            pl.semaphore_signal(
                barrier,
                inc=1,
                device_id=at(sp, lax.rem(fs + a, nfs), lax.rem(tp + b, ntp)),
                device_id_type=MESH,
            )

    @pl.when(jnp.logical_not(first))
    def _():
        pl.semaphore_signal(barrier, inc=1, device_id=at(sp - 1, fs, tp), device_id_type=MESH)

    @pl.when(jnp.logical_not(last))
    def _():
        pl.semaphore_signal(barrier, inc=1, device_id=at(sp + 1, fs, tp), device_id_type=MESH)

    own_weights = [
        pltpu.make_async_copy(wstate_hbm, wstate.at[tp], local_sem.at[0]),
        pltpu.make_async_copy(wconv_hbm, wconv.at[tp], local_sem.at[1]),
    ]
    for copy in own_weights:
        copy.start()

    ends = jnp.minimum(sp, 1) + jnp.minimum(nsp - 1 - sp, 1)
    pl.semaphore_wait(barrier, nfs * ntp - 1 + ends)

    def remote(src, dst, ss, rs, device):
        return pltpu.make_async_remote_copy(
            src_ref=src, dst_ref=dst, send_sem=ss, recv_sem=rs, device_id=device, device_id_type=MESH
        )

    nxt = at(jnp.minimum(sp + 1, nsp - 1), fs, tp)
    tail = pl.ds(length - HALO, HALO)
    halos = [
        remote(src.at[0, tail, :], dst, halo_ss.at[k], halo_rs.at[k], nxt)
        for k, (src, dst) in enumerate(
            (
                (writes_ref, write_halo),
                (reads_ref, read_halo),
                (head_ref, head_halo),
                (inner_ref, inner_halo),
                (value_ref, value_halo),
            )
        )
    ]

    @pl.when(jnp.logical_not(last))
    def _():
        for copy in halos:
            copy.start()

    weights = []
    for b in range(1, ntp):
        other = at(sp, fs, lax.rem(tp + b, ntp))
        weights.append(
            remote(wconv_hbm, wconv.at[tp], weight_ss.at[b - 1, 0], weight_rs.at[b - 1, 0], other)
        )
        weights.append(
            remote(wstate_hbm, wstate.at[tp], weight_ss.at[b - 1, 1], weight_rs.at[b - 1, 1], other)
        )
    for copy in weights:
        copy.start()

    logits = step_ref[0] + offset_ref[...]
    dt = jnp.maximum(logits, 0.0) + jnp.log1p(jnp.exp(-jnp.abs(logits)))
    fall = spike_ref[...] - dt * jnp.exp(rate_ref[...])
    rows = lax.broadcasted_iota(jnp.int32, (length, length), 0)
    cols = lax.broadcasted_iota(jnp.int32, (length, length), 1)
    causal = cols <= rows
    rising = jnp.dot(
        causal.astype(F32), fall, precision=HIGH, preferred_element_type=F32
    )
    rising_t = rising.T
    dt_t = dt.T
    grow = jnp.exp(rising)
    left = dt * jnp.exp(rising[length - 1 : length] - rising)
    spread = (
        lax.broadcasted_iota(jnp.int32, (heads, width), 1) // channels
        == lax.broadcasted_iota(jnp.int32, (heads, width), 0)
    ).astype(BF16)
    stacked = jnp.concatenate([grow, left], axis=0)
    coarse = stacked.astype(BF16)
    fine = (stacked - coarse.astype(F32)).astype(BF16)
    wide = mm(coarse, spread) + mm(fine, spread)
    grow_wide, left_wide = wide[:length], wide[length:]
    last_wide = grow_wide[length - 1 : length]

    @pl.when(first)
    def _():
        for ref in (head_halo, write_halo, read_halo, inner_halo, value_halo):
            ref[...] = jnp.zeros_like(ref)

    @pl.when(jnp.logical_not(first))
    def _():
        for copy in halos:
            copy.wait_recv()

    def causal_filter(pad, stream, before, taps):
        span = taps.shape[0]
        pad[0:HALO, :] = before
        pad[HALO : HALO + length, :] = stream
        total = None
        for k in range(span):
            start = HALO - (span - 1) + k
            term = pad[start : start + length, :] * taps[k : k + 1]
            total = term if total is None else total + term
        return total

    writes = silu(
        causal_filter(
            group_pad, writes_ref[0].astype(F32), write_halo[...].astype(F32), write_taps[...].astype(F32)
        )
    )
    filtered = silu(
        causal_filter(
            head_pad, head_ref[0].astype(F32), head_halo[...].astype(F32), head_taps[...].astype(F32)
        )
    )
    writes_t = [
        writes[:, g * STATE : (g + 1) * STATE].T.astype(BF16) for g in range(groups)
    ]
    weighted = (filtered * left_wide).astype(BF16)
    for g in range(groups):
        piece = mm(writes_t[g], weighted[:, g * gw : (g + 1) * gw])
        for i in range(per_group):
            local_state[g * per_group + i] = piece[:, i * LANES : (i + 1) * LANES]

    chain = [
        remote(state_send.at[i], state_recv.at[i], state_ss.at[i], state_rs.at[i], nxt)
        for i in range(chunks)
    ]

    @pl.when(first)
    def _():
        for i in range(chunks):
            state_send[i] = local_state[i].astype(BF16)
        for copy in chain:
            copy.start()

    product = inner_ref[0].astype(F32) * value_ref[0].astype(F32)
    before = inner_halo[...].astype(F32) * value_halo[...].astype(F32)
    convolved = causal_filter(conv_pad, product, before, conv_taps[...].astype(F32))
    conv_rows = (outer_ref[0].astype(F32) * convolved).astype(BF16)
    conv_send[...] = conv_rows
    conv_copies = []
    for a in range(1, nfs):
        conv_copies.append(
            remote(
                conv_send,
                conv_recv.at[slot, tp],
                conv_ss.at[a],
                conv_rs.at[slot, tp],
                at(sp, lax.rem(fs + a, nfs), dest),
            )
        )
    for copy in conv_copies:
        copy.start()
    conv_home = remote(
        conv_send, conv_recv.at[slot, tp], conv_ss.at[0], conv_rs.at[slot, tp], at(sp, fs, dest)
    )

    @pl.when(dest == tp)
    def _():
        conv_recv[slot, tp] = conv_rows

    @pl.when(dest != tp)
    def _():
        conv_home.start()

    reads = silu(
        causal_filter(
            group_pad, reads_ref[0].astype(F32), read_halo[...].astype(F32), read_taps[...].astype(F32)
        )
    ).astype(BF16)
    filtered16 = filtered.astype(BF16)
    lane_head = lax.broadcasted_iota(jnp.int32, (length, LANES), 1) // channels
    for g in range(groups):
        scores = jnp.where(causal, mm(reads[:, g * STATE : (g + 1) * STATE], writes_t[g]), 0.0)
        for i in range(g * per_group, (g + 1) * per_group):
            block = filtered16[:, i * LANES : (i + 1) * LANES]
            total = None
            for r in range(hpl):
                h = i * hpl + r
                gaps = jnp.minimum(rising[:, h : h + 1] - rising_t[h : h + 1, :], 0.0)
                mixed = (scores * jnp.exp(gaps) * dt_t[h : h + 1, :]).astype(BF16)
                part = mm(mixed, block)
                total = part if total is None else jnp.where(lane_head == r, part, total)
            inside[:, i * LANES : (i + 1) * LANES] = total

    def branch_copy(g, a):
        return remote(
            branch_send.at[g],
            branch_recv.at[slot, tp, g],
            branch_ss.at[g, a],
            branch_rs.at[slot, tp, g],
            at(sp, lax.rem(fs + a, nfs), dest),
        )

    for g in range(groups):
        for i in range(g * per_group, (g + 1) * per_group):
            lanes = slice(i * LANES, (i + 1) * LANES)

            @pl.when(jnp.logical_not(first))
            def _():
                chain[i].wait_recv()
                incoming = state_recv[i]

                @pl.when(jnp.logical_not(last))
                def _():
                    state_send[i] = (
                        incoming.astype(F32) * last_wide[:, lanes] + local_state[i]
                    ).astype(BF16)
                    chain[i].start()

                inside[:, lanes] += (
                    mm(reads[:, g * STATE : (g + 1) * STATE], incoming) * grow_wide[:, lanes]
                )

        span = slice(g * gw, (g + 1) * gw)
        gated = inside[:, span] * silu(gate_ref[0, :, span].astype(F32))
        power = jnp.mean(gated * gated, axis=1, keepdims=True)
        normed = (gated * lax.rsqrt(power + EPS) * scale_ref[:, span]).astype(BF16)
        branch_send[g] = normed
        for a in range(1, nfs):
            branch_copy(g, a).start()

        @pl.when(dest == tp)
        def _():
            branch_recv[slot, tp, g] = normed

        @pl.when(dest != tp)
        def _():
            branch_copy(g, 0).start()

    for copy in own_weights:
        copy.wait()
    for copy in weights:
        copy.wait_recv()

    def local_source(j, c):
        return jnp.logical_and(fs == tp * per_tp + j, tp == c)

    for c in range(ntp):
        for j in range(per_tp):

            @pl.when(jnp.logical_not(local_source(j, c)))
            def _():
                remote(
                    conv_send, conv_recv.at[j, c], conv_ss.at[0], conv_rs.at[j, c], at(sp, fs, dest)
                ).wait_recv()

            term = mm(conv_recv[j, c], wconv[c])
            if c == 0:
                acc[j] = term
            else:
                acc[j] += term
    for g in range(groups):
        for c in range(ntp):
            for j in range(per_tp):

                @pl.when(jnp.logical_not(local_source(j, c)))
                def _():
                    remote(
                        branch_send.at[g],
                        branch_recv.at[j, c, g],
                        branch_ss.at[g, 0],
                        branch_rs.at[j, c, g],
                        at(sp, fs, dest),
                    ).wait_recv()

                acc[j] += mm(branch_recv[j, c, g], wstate[c, g * gw : (g + 1) * gw, :])
    for j in range(per_tp):
        out_ref[j] = acc[j].astype(BF16)

    @pl.when(jnp.logical_not(last))
    def _():
        for copy in halos:
            copy.wait_send()
        for copy in chain:
            copy.wait_send()

    for copy in weights:
        copy.wait_send()
    for copy in conv_copies:
        copy.wait_send()
    for g in range(groups):
        for a in range(1, nfs):
            branch_copy(g, a).wait_send()

    @pl.when(dest != tp)
    def _():
        conv_home.wait_send()
        for g in range(groups):
            branch_copy(g, 0).wait_send()


def per_device(sizes, *arrays):
    (
        gate,
        head,
        writes,
        reads,
        steps,
        offset,
        rates,
        spikes,
        head_taps,
        write_taps,
        read_taps,
        scale,
        outer,
        inner,
        value,
        conv_taps,
        wstate,
        wconv,
    ) = arrays
    nsp, nfs, ntp = sizes
    length, width = head.shape[1:]
    group_width = writes.shape[2]
    groups = group_width // STATE
    conv_width = inner.shape[2]
    features = wstate.shape[1]
    per_tp = nfs // ntp
    chunks = width // LANES
    vm = pl.BlockSpec(memory_space=pltpu.VMEM)
    hbm = pl.BlockSpec(memory_space=pl.ANY)
    dma = pltpu.SemaphoreType.DMA
    return pl.pallas_call(
        functools.partial(kernel, sizes),
        out_shape=jax.ShapeDtypeStruct((per_tp, length, features), BF16),
        in_specs=[vm] * 16 + [hbm] * 2,
        out_specs=vm,
        scratch_shapes=[
            pltpu.VMEM((HALO, width), BF16),
            pltpu.VMEM((HALO, group_width), BF16),
            pltpu.VMEM((HALO, group_width), BF16),
            pltpu.VMEM((HALO, conv_width), BF16),
            pltpu.VMEM((HALO, conv_width), BF16),
            pltpu.VMEM((HALO + length, width), F32),
            pltpu.VMEM((HALO + length, group_width), F32),
            pltpu.VMEM((HALO + length, conv_width), F32),
            pltpu.VMEM((chunks, STATE, LANES), F32),
            pltpu.VMEM((chunks, STATE, LANES), BF16),
            pltpu.VMEM((chunks, STATE, LANES), BF16),
            pltpu.VMEM((length, width), F32),
            pltpu.VMEM((groups, length, width // groups), BF16),
            pltpu.VMEM((per_tp, ntp, groups, length, width // groups), BF16),
            pltpu.VMEM((length, conv_width), BF16),
            pltpu.VMEM((per_tp, ntp, length, conv_width), BF16),
            pltpu.VMEM((ntp, width, features), BF16),
            pltpu.VMEM((ntp, conv_width, features), BF16),
            pltpu.VMEM((per_tp, length, features), F32),
            dma((5,)),
            dma((5,)),
            dma((chunks,)),
            dma((chunks,)),
            dma((groups, nfs)),
            dma((per_tp, ntp, groups)),
            dma((nfs,)),
            dma((per_tp, ntp)),
            dma((ntp - 1, 2)),
            dma((ntp - 1, 2)),
            dma((2,)),
        ],
        compiler_params=pltpu.CompilerParams(collective_id=0, has_side_effects=True),
    )(
        gate,
        head,
        writes,
        reads,
        steps,
        offset[None],
        rates[None],
        spikes,
        head_taps,
        write_taps,
        read_taps,
        scale[None],
        outer,
        inner,
        value,
        conv_taps,
        wstate,
        wconv,
    )


def solution(mesh):
    sizes = tuple(mesh.shape[name] for name in ("sp", "fs", "tp"))
    return jax.shard_map(
        functools.partial(per_device, sizes),
        mesh=mesh,
        in_specs=(
            P("fs", "sp", "tp"),
            P("fs", "sp", "tp"),
            P("fs", "sp", "tp"),
            P("fs", "sp", "tp"),
            P("fs", "sp", "tp"),
            P("tp"),
            P("tp"),
            P("sp", "tp"),
            P(None, "tp"),
            P(None, "tp"),
            P(None, "tp"),
            P("tp"),
            P("fs", "sp", "tp"),
            P("fs", "sp", "tp"),
            P("fs", "sp", "tp"),
            P(None, "tp"),
            P("tp", "fs"),
            P("tp", "fs"),
        ),
        out_specs=P("tp", "sp", "fs"),
        check_vma=False,
    )
```

time: 108 us -> 32.1 us (0.30); the launches traced: 106 us -> 31.9 us
  waiting for transfers between devices: 45.5 us -> 0 us
  Pallas kernels: 0 us -> 28 us
  between operations: 15.2 us -> 0.01 us
  blocking collectives: 14.4 us -> 0 us
  other arithmetic: 9.86 us -> 0 us
  matrix products: 9.16 us -> 0 us
  local copies, waits for them, and re-layouts: 10.3 us -> 3.83 us
  starting transfers between devices: 1.54 us -> 0 us
    all_gather x2 -> x0, waiting for transfers between devices: 36.5 us -> none  [the longest x1 19.8 us: entering(): lax.all_gather(part.astype(kind), axis)]
    pallas_call x0 -> x1, Pallas kernels: none -> 28 us  [per_device(): pl.pallas_call(functools.partial(kernel, sizes), out_shape=jax.ShapeDtype...]
    all_gather x2 -> x0, blocking collectives: 14.4 us -> none  [the longest x1 8.33 us: per_device(): lax.all_gather(conv_rows, 'fs', axis=0, tiled=True)]
    dot_general x7 -> x0, matrix products: 9.16 us -> none  [the longest x1 2.77 us: per_device(): jnp.dot(lax.all_gather(state_rows, 'fs', axis=0, tiled=True), state_outpu...]
    reduce_scatter x2 -> x0, waiting for transfers between devices: 8.9 us -> none  [the longest x1 8.88 us: per_device(): lax.psum_scatter(state_terms.astype(jnp.bfloat16), 'tp', scatter_dimensio...]
    unnamed x42 -> x5, local copies, waits for them, and re-layouts: 8.48 us -> 3.83 us
    select_n x4 -> x0, other arithmetic: 4.4 us -> none  [turn(): return jax.tree.map(lambda a, b: jnp.where(reached, a, b), new, before)]
    convert_element_type x7 -> x0, other arithmetic: 2.88 us -> none  [the longest x1 1.8 us: per_device(): return summed.astype(jnp.bfloat16).reshape(-1, length, summed.shape[1])]
  transfers between devices with their start and end apart: 5 -> 0, of which waited for: 3 -> 0; matrix products, arithmetic and copies ran while one was open for 7% -> 0% of each run, Pallas kernels for 0% -> 0%
where the time goes in v1:
time: 32.1 us; the launch traced here: 31.9 us
  Pallas kernels  28 us (87%)
  local copies, waits for them, and re-layouts  3.83 us (12%)
    pallas_call x1, Pallas kernels, per_device(): pl.pallas_call(functools.partial(kernel, sizes), out_shape=jax.ShapeDtype...  28 us
    unnamed x5, local copies, waits for them, and re-layouts  3.83 us

profile of v1, /device:TPU:25, one launch (start us, length us, event | category | flops | bytes accessed | tf_op | source)
XLA Modules:
  0.0 31.9 jit_solution(13649966440256522703)
XLA Ops:
  0.0 0.0 copy-start
  0.0 1.4 %copy.19.step_ref = f32[1,128,16]{2,1,0:T(8,128)} copy(f32[1,128,16]{1,2,0:T(8,128)} %param.22) | data formatting | bytes 16384 | tf_op args[4]
  1.4 0.0 copy-done
  1.4 0.7 %copy.20.spike_ref = f32[128,16]{1,0:T(8,128)} copy(f32[128,16]{0,1:T(8,128)S(1)} %copy-done) | data formatting | bytes 16384 | tf_op args[7]
  2.2 28.0 %shard_map.172 = bf16[2,128,512]{2,1,0:T(8,128)(2,1)} custom-call(bf16[1,128,1024]{2,1,0:T(8,128)(2,1)} %gate_ref.1, bf16[1,128,1024]{2,1,0:T(8,128)(2,1)} %head_ref.1, bf16[1,128,256]{2,1,0:T(8,128)(2,1)} %writes_ref.1, bf16[1,128,256]{2,1,0:T(8,128)(2,1)} %reads_ref.1, f32[1,128,16]{2,1,0:T(8,128)} %copy.19.step_ref, f32[1,16]{1,0:T(1,128)} %bitcast.4, ...), custom_call_target="tpu_custom_call" | custom-call | tf_op jit(solution)/shard_map/pallas_call | solution.py:432
  30.2 1.7 %copy.22 = bf16[2,128,512]{2,1,0:T(8,128)(2,1)} copy(bf16[2,128,512]{2,1,0:T(8,128)(2,1)} %shard_map.172) | data formatting | bytes 524288
Async XLA Ops:
  0.0 1.4 %copy-start = (f32[128,16]{0,1:T(8,128)S(1)}, f32[128,16]{0,1:T(8,128)}, u32[]{:S(2)}) copy-start(f32[128,16]{0,1:T(8,128)} %param.25) | copy-start | bytes 24580

commit v2 on v1

--- a/solution.py
+++ b/solution.py
@@ -27,10 +27,10 @@
 
 def kernel(
     sizes,
-    gate_ref,
-    head_ref,
-    writes_ref,
-    reads_ref,
+    gate_hbm,
+    head_hbm,
+    writes_hbm,
+    reads_hbm,
     step_ref,
     offset_ref,
     rate_ref,
@@ -39,13 +39,20 @@
     write_taps,
     read_taps,
     scale_ref,
-    outer_ref,
-    inner_ref,
-    value_ref,
+    outer_hbm,
+    inner_hbm,
+    value_hbm,
     conv_taps,
     wstate_hbm,
     wconv_hbm,
     out_ref,
+    gate_ref,
+    head_ref,
+    writes_ref,
+    reads_ref,
+    outer_ref,
+    inner_ref,
+    value_ref,
     head_halo,
     write_halo,
     read_halo,
@@ -57,20 +64,28 @@
     local_state,
     state_send,
     state_recv,
-    inside,
     branch_send,
     branch_recv,
+    norm_send,
+    norm_recv,
     conv_send,
     conv_recv,
     wstate,
     wconv,
     acc,
+    part,
+    inside,
+    input_sem,
     halo_ss,
     halo_rs,
     state_ss,
     state_rs,
     branch_ss,
     branch_rs,
+    half_ss,
+    half_rs,
+    norm_ss,
+    norm_rs,
     conv_ss,
     conv_rs,
     weight_ss,
@@ -80,7 +95,7 @@
     nsp, nfs, ntp = sizes
     sp, fs, tp = lax.axis_index("sp"), lax.axis_index("fs"), lax.axis_index("tp")
     length, width = head_ref.shape[1:]
-    heads = step_ref.shape[2]
+    heads = step_ref.shape[1]
     channels = width // heads
     group_width = writes_ref.shape[2]
     groups = group_width // STATE
@@ -90,6 +105,10 @@
     chunks = width // LANES
     per_group = chunks // groups
     hpl = LANES // channels
+    per_unit = min(2, per_group)
+    units = chunks // per_unit
+    unit_width = per_unit * LANES
+    half = length // 2
     dest = fs // per_tp
     slot = lax.rem(fs, per_tp)
     first, last = sp == 0, sp == nsp - 1
@@ -117,6 +136,23 @@
     def _():
         pl.semaphore_signal(barrier, inc=1, device_id=at(sp + 1, fs, tp), device_id_type=MESH)
 
+    inputs = [
+        pltpu.make_async_copy(src, dst, input_sem.at[k])
+        for k, (src, dst) in enumerate(
+            (
+                (writes_hbm, writes_ref),
+                (reads_hbm, reads_ref),
+                (head_hbm, head_ref),
+                (inner_hbm, inner_ref),
+                (value_hbm, value_ref),
+                (outer_hbm, outer_ref),
+                (gate_hbm, gate_ref),
+            )
+        )
+    ]
+    for copy in inputs:
+        copy.start()
+
     own_weights = [
         pltpu.make_async_copy(wstate_hbm, wstate.at[tp], local_sem.at[0]),
         pltpu.make_async_copy(wconv_hbm, wconv.at[tp], local_sem.at[1]),
@@ -125,6 +161,8 @@
         copy.start()
 
     ends = jnp.minimum(sp, 1) + jnp.minimum(nsp - 1 - sp, 1)
+    for copy in inputs:
+        copy.wait()
     pl.semaphore_wait(barrier, nfs * ntp - 1 + ends)
 
     def remote(src, dst, ss, rs, device):
@@ -164,28 +202,30 @@
     for copy in weights:
         copy.start()
 
-    logits = step_ref[0] + offset_ref[...]
-    dt = jnp.maximum(logits, 0.0) + jnp.log1p(jnp.exp(-jnp.abs(logits)))
-    fall = spike_ref[...] - dt * jnp.exp(rate_ref[...])
+    def column(ref):
+        return jnp.broadcast_to(ref[...], (length, heads)).T
+
+    logits = step_ref[0] + column(offset_ref)
+    dt_t = jnp.maximum(logits, 0.0) + jnp.log1p(jnp.exp(-jnp.abs(logits)))
+    fall = spike_ref[...] - dt_t * jnp.exp(column(rate_ref))
     rows = lax.broadcasted_iota(jnp.int32, (length, length), 0)
     cols = lax.broadcasted_iota(jnp.int32, (length, length), 1)
     causal = cols <= rows
-    rising = jnp.dot(
-        causal.astype(F32), fall, precision=HIGH, preferred_element_type=F32
+    rising_t = jnp.dot(
+        fall, (rows <= cols).astype(F32), precision=HIGH, preferred_element_type=F32
     )
-    rising_t = rising.T
-    dt_t = dt.T
-    grow = jnp.exp(rising)
-    left = dt * jnp.exp(rising[length - 1 : length] - rising)
+    rising = rising_t.T
+    grow = jnp.exp(rising_t)
+    left = dt_t * jnp.exp(rising_t[:, length - 1 : length] - rising_t)
+    stacked = jnp.concatenate([grow, left], axis=0)
+    coarse = stacked.astype(BF16).astype(F32)
+    split = jnp.concatenate([coarse, stacked - coarse], axis=0).T.astype(BF16)
     spread = (
-        lax.broadcasted_iota(jnp.int32, (heads, width), 1) // channels
-        == lax.broadcasted_iota(jnp.int32, (heads, width), 0)
+        lax.broadcasted_iota(jnp.int32, (4 * heads, 2 * width), 1) // channels
+        == lax.broadcasted_iota(jnp.int32, (4 * heads, 2 * width), 0) % (2 * heads)
     ).astype(BF16)
-    stacked = jnp.concatenate([grow, left], axis=0)
-    coarse = stacked.astype(BF16)
-    fine = (stacked - coarse.astype(F32)).astype(BF16)
-    wide = mm(coarse, spread) + mm(fine, spread)
-    grow_wide, left_wide = wide[:length], wide[length:]
+    wide = mm(split, spread)
+    grow_wide, left_wide = wide[:, :width], wide[:, width:]
     last_wide = grow_wide[length - 1 : length]
 
     @pl.when(first)
@@ -286,20 +326,36 @@
                 h = i * hpl + r
                 gaps = jnp.minimum(rising[:, h : h + 1] - rising_t[h : h + 1, :], 0.0)
                 mixed = (scores * jnp.exp(gaps) * dt_t[h : h + 1, :]).astype(BF16)
-                part = mm(mixed, block)
-                total = part if total is None else jnp.where(lane_head == r, part, total)
+                one = mm(mixed, block)
+                total = one if total is None else jnp.where(lane_head == r, one, total)
             inside[:, i * LANES : (i + 1) * LANES] = total
 
-    def branch_copy(g, a):
+    home = dest == tp
+    xfs = fs + 1 - 2 * lax.rem(fs, 2)
+    yfs = lax.rem(fs + 2, nfs)
+    pfs = nfs - 1 - fs
+
+    def branch_copy(u, k, f):
         return remote(
-            branch_send.at[g],
-            branch_recv.at[slot, tp, g],
-            branch_ss.at[g, a],
-            branch_rs.at[slot, tp, g],
-            at(sp, lax.rem(fs + a, nfs), dest),
+            branch_send.at[u],
+            branch_recv.at[slot, tp, u],
+            branch_ss.at[u, k],
+            branch_rs.at[slot, tp, u],
+            at(sp, f, dest),
+        )
+
+    def norm_copy(g, k, f):
+        return remote(
+            norm_send.at[g],
+            norm_recv.at[slot, tp, g],
+            norm_ss.at[g, k],
+            norm_rs.at[slot, tp, g],
+            at(sp, f, dest),
         )
 
     for g in range(groups):
+        span = slice(g * gw, (g + 1) * gw)
+        power = jnp.zeros((length, LANES), F32)
         for i in range(g * per_group, (g + 1) * per_group):
             lanes = slice(i * LANES, (i + 1) * LANES)
 
@@ -319,21 +375,38 @@
                     mm(reads[:, g * STATE : (g + 1) * STATE], incoming) * grow_wide[:, lanes]
                 )
 
-        span = slice(g * gw, (g + 1) * gw)
-        gated = inside[:, span] * silu(gate_ref[0, :, span].astype(F32))
-        power = jnp.mean(gated * gated, axis=1, keepdims=True)
-        normed = (gated * lax.rsqrt(power + EPS) * scale_ref[:, span]).astype(BF16)
-        branch_send[g] = normed
-        for a in range(1, nfs):
-            branch_copy(g, a).start()
-
-        @pl.when(dest == tp)
+            gated = inside[:, lanes] * silu(gate_ref[0, :, lanes].astype(F32))
+            power = power + gated * gated
+            u, at_lane = i // per_unit, (i % per_unit) * LANES
+            scaled = (gated * scale_ref[:, lanes]).astype(BF16)
+            branch_send[u, 0, :, at_lane : at_lane + LANES] = scaled[:half]
+            branch_send[u, 1, :, at_lane : at_lane + LANES] = scaled[half:]
+            if i % per_unit == per_unit - 1:
+                branch_copy(u, 1, xfs).start()
+                branch_copy(u, 2, yfs).start()
+
+                @pl.when(home)
+                def _():
+                    branch_recv[slot, tp, u] = branch_send[u]
+
+                @pl.when(jnp.logical_not(home))
+                def _():
+                    branch_copy(u, 0, fs).start()
+
+        factor = lax.rsqrt(jnp.sum(power, axis=1, keepdims=True) / gw + EPS)
+        factor = jnp.broadcast_to(factor, (length, LANES)).T[:8]
+        norm_send[g] = factor
+        norm_copy(g, 1, xfs).start()
+        norm_copy(g, 2, yfs).start()
+        norm_copy(g, 3, pfs).start()
+
+        @pl.when(home)
         def _():
-            branch_recv[slot, tp, g] = normed
-
-        @pl.when(dest != tp)
+            norm_recv[slot, tp, g] = factor
+
+        @pl.when(jnp.logical_not(home))
         def _():
-            branch_copy(g, 0).start()
+            norm_copy(g, 0, fs).start()
 
     for copy in own_weights:
         copy.wait()
@@ -357,21 +430,81 @@
                 acc[j] = term
             else:
                 acc[j] += term
-    for g in range(groups):
+    own = lax.rem(fs, 2)
+    side = jnp.where(home, 1 - own, own)
+    upper = jnp.where(home, 0, 1)
+    onward = at(sp, jnp.where(home, yfs, xfs), tp)
+
+    def forward(c, u):
+        return remote(
+            branch_recv.at[side, c, u, upper],
+            branch_recv.at[side, c, u, upper],
+            half_ss.at[c, u],
+            half_rs.at[upper, c, u],
+            onward,
+        )
+
+    def arrived(j, c, u):
+        remote(
+            branch_send.at[u],
+            branch_recv.at[j, c, u],
+            branch_ss.at[u, 0],
+            branch_rs.at[j, c, u],
+            at(sp, xfs, dest),
+        ).wait_recv()
+
+    for u in range(units):
         for c in range(ntp):
-            for j in range(per_tp):
-
-                @pl.when(jnp.logical_not(local_source(j, c)))
-                def _():
-                    remote(
-                        branch_send.at[g],
-                        branch_recv.at[j, c, g],
-                        branch_ss.at[g, 0],
-                        branch_rs.at[j, c, g],
-                        at(sp, fs, dest),
-                    ).wait_recv()
-
-                acc[j] += mm(branch_recv[j, c, g], wstate[c, g * gw : (g + 1) * gw, :])
+            arrived(side, c, u)
+            forward(c, u).start()
+
+    def project(j, u, c):
+        rows = branch_recv[j, c, u].reshape(length, unit_width)
+        term = mm(rows, wstate[c, u * unit_width : (u + 1) * unit_width, :])
+        if (u * per_unit) % per_group == 0:
+            part[c] = term
+        else:
+            part[c] += term
+
+    def finish(j, g, c):
+        @pl.when(jnp.logical_not(local_source(j, c)))
+        def _():
+            remote(
+                norm_send.at[g],
+                norm_recv.at[j, c, g],
+                norm_ss.at[g, 0],
+                norm_rs.at[j, c, g],
+                at(sp, xfs, dest),
+            ).wait_recv()
+
+        turned = jnp.broadcast_to(norm_recv[j, c, g][:1], (LANES, length)).T
+        acc[j] += part[c] * turned[:, :1]
+
+    per_norm = per_group // per_unit
+    for j, straight in ((side, True), (1 - side, False)):
+        for g in range(groups):
+            for u in range(g * per_norm, (g + 1) * per_norm):
+                for c in range(ntp):
+                    if not straight:
+
+                        @pl.when(jnp.logical_and(home, tp != c))
+                        def _():
+                            arrived(j, c, u)
+
+                        @pl.when(jnp.logical_not(home))
+                        def _():
+                            for h in range(2):
+                                remote(
+                                    branch_send.at[u, h],
+                                    branch_recv.at[j, c, u, h],
+                                    half_ss.at[c, u],
+                                    half_rs.at[h, c, u],
+                                    onward,
+                                ).wait_recv()
+
+                    project(j, u, c)
+            for c in range(ntp):
+                finish(j, g, c)
     for j in range(per_tp):
         out_ref[j] = acc[j].astype(BF16)
 
@@ -386,15 +519,23 @@
         copy.wait_send()
     for copy in conv_copies:
         copy.wait_send()
+    for u in range(units):
+        branch_copy(u, 1, xfs).wait_send()
+        branch_copy(u, 2, yfs).wait_send()
+        for c in range(ntp):
+            forward(c, u).wait_send()
     for g in range(groups):
-        for a in range(1, nfs):
-            branch_copy(g, a).wait_send()
-
-    @pl.when(dest != tp)
+        norm_copy(g, 1, xfs).wait_send()
+        norm_copy(g, 2, yfs).wait_send()
+        norm_copy(g, 3, pfs).wait_send()
+
+    @pl.when(jnp.logical_not(home))
     def _():
         conv_home.wait_send()
+        for u in range(units):
+            branch_copy(u, 0, fs).wait_send()
         for g in range(groups):
-            branch_copy(g, 0).wait_send()
+            norm_copy(g, 0, fs).wait_send()
 
 
 def per_device(sizes, *arrays):
@@ -426,15 +567,27 @@
     features = wstate.shape[1]
     per_tp = nfs // ntp
     chunks = width // LANES
+    half = length // 2
+    per_unit = min(2, chunks // groups)
+    units = chunks // per_unit
+    if (nfs, ntp) != (4, 2):
+        raise ValueError('unsupported mesh')
     vm = pl.BlockSpec(memory_space=pltpu.VMEM)
     hbm = pl.BlockSpec(memory_space=pl.ANY)
     dma = pltpu.SemaphoreType.DMA
     return pl.pallas_call(
         functools.partial(kernel, sizes),
         out_shape=jax.ShapeDtypeStruct((per_tp, length, features), BF16),
-        in_specs=[vm] * 16 + [hbm] * 2,
+        in_specs=[hbm] * 4 + [vm] * 8 + [hbm] * 3 + [vm] + [hbm] * 2,
         out_specs=vm,
         scratch_shapes=[
+            pltpu.VMEM((1, length, width), BF16),
+            pltpu.VMEM((1, length, width), BF16),
+            pltpu.VMEM((1, length, group_width), BF16),
+            pltpu.VMEM((1, length, group_width), BF16),
+            pltpu.VMEM((1, length, conv_width), BF16),
+            pltpu.VMEM((1, length, conv_width), BF16),
+            pltpu.VMEM((1, length, conv_width), BF16),
             pltpu.VMEM((HALO, width), BF16),
             pltpu.VMEM((HALO, group_width), BF16),
             pltpu.VMEM((HALO, group_width), BF16),
@@ -446,18 +599,26 @@
             pltpu.VMEM((chunks, STATE, LANES), F32),
             pltpu.VMEM((chunks, STATE, LANES), BF16),
             pltpu.VMEM((chunks, STATE, LANES), BF16),
-            pltpu.VMEM((length, width), F32),
-            pltpu.VMEM((groups, length, width // groups), BF16),
-            pltpu.VMEM((per_tp, ntp, groups, length, width // groups), BF16),
+            pltpu.VMEM((units, 2, half, width // units), BF16),
+            pltpu.VMEM((per_tp, ntp, units, 2, half, width // units), BF16),
+            pltpu.VMEM((groups, 8, length), F32),
+            pltpu.VMEM((per_tp, ntp, groups, 8, length), F32),
             pltpu.VMEM((length, conv_width), BF16),
             pltpu.VMEM((per_tp, ntp, length, conv_width), BF16),
             pltpu.VMEM((ntp, width, features), BF16),
             pltpu.VMEM((ntp, conv_width, features), BF16),
             pltpu.VMEM((per_tp, length, features), F32),
+            pltpu.VMEM((ntp, length, features), F32),
+            pltpu.VMEM((length, width), F32),
+            dma((7,)),
             dma((5,)),
             dma((5,)),
             dma((chunks,)),
             dma((chunks,)),
+            dma((units, 3)),
+            dma((per_tp, ntp, units)),
+            dma((ntp, units)),
+            dma((2, ntp, units)),
             dma((groups, nfs)),
             dma((per_tp, ntp, groups)),
             dma((nfs,)),
@@ -472,10 +633,10 @@
         head,
         writes,
         reads,
-        steps,
+        jnp.swapaxes(steps, 1, 2),
         offset[None],
         rates[None],
-        spikes,
+        spikes.T,
         head_taps,
         write_taps,
         read_taps,

time: 32.1 us -> 28.2 us (0.88)
  local copies, waits for them, and re-layouts: 3.83 us -> 1.67 us
  Pallas kernels: 28 us -> 26.2 us
    unnamed x5 -> x1, local copies, waits for them, and re-layouts: 3.83 us -> 1.67 us
    pallas_call x1, Pallas kernels: 28 us -> 26.2 us  [per_device(): pl.pallas_call(functools.partial(kernel, sizes), out_shape=jax.ShapeDtype...]
where the time goes in v2:
time: 28.2 us; the launch traced here: 27.8 us
  Pallas kernels  26.2 us (93%)
  local copies, waits for them, and re-layouts  1.67 us (6%)
    pallas_call x1, Pallas kernels, per_device(): pl.pallas_call(functools.partial(kernel, sizes), out_shape=jax.ShapeDtype...  26.2 us
    unnamed x1, local copies, waits for them, and re-layouts  1.67 us

profile of v2, /device:TPU:25, one launch (start us, length us, event | category | flops | bytes accessed | tf_op | source)
XLA Modules:
  0.0 27.8 jit_solution(3453538089593755730)
XLA Ops:
  0.0 26.2 %shard_map.172 = bf16[2,128,512]{2,1,0:T(8,128)(2,1)} custom-call(bf16[1,128,1024]{2,1,0:T(8,128)(2,1)} %gate_hbm.1, bf16[1,128,1024]{2,1,0:T(8,128)(2,1)} %head_hbm.1, bf16[1,128,256]{2,1,0:T(8,128)(2,1)} %writes_hbm.1, bf16[1,128,256]{2,1,0:T(8,128)(2,1)} %reads_hbm.1, f32[1,16,128]{2,1,0:T(8,128)} %bitcast.5, f32[1,16]{1,0:T(1,128)} %bitcast.8, ...), custom_call_target="tpu_custom_call" | custom-call | tf_op jit(solution)/shard_map/pallas_call | solution.py:578
  26.2 1.7 %copy.20 = bf16[2,128,512]{2,1,0:T(8,128)(2,1)} copy(bf16[2,128,512]{2,1,0:T(8,128)(2,1)} %shard_map.172) | data formatting | bytes 524288

commit v3 on v2

--- a/solution.py
+++ b/solution.py
@@ -22,7 +22,7 @@
 
 
 def silu(v):
-    return v / (1.0 + jnp.exp(-v))
+    return 0.5 * v * (1.0 + jnp.tanh(0.5 * v))
 
 
 def kernel(
@@ -59,7 +59,10 @@
     inner_halo,
     value_halo,
     head_pad,
-    group_pad,
+    write_pad,
+    read_pad,
+    head_act,
+    write_act,
     conv_pad,
     local_state,
     state_send,
@@ -190,18 +193,6 @@
         for copy in halos:
             copy.start()
 
-    weights = []
-    for b in range(1, ntp):
-        other = at(sp, fs, lax.rem(tp + b, ntp))
-        weights.append(
-            remote(wconv_hbm, wconv.at[tp], weight_ss.at[b - 1, 0], weight_rs.at[b - 1, 0], other)
-        )
-        weights.append(
-            remote(wstate_hbm, wstate.at[tp], weight_ss.at[b - 1, 1], weight_rs.at[b - 1, 1], other)
-        )
-    for copy in weights:
-        copy.start()
-
     def column(ref):
         return jnp.broadcast_to(ref[...], (length, heads)).T
 
@@ -220,69 +211,77 @@
     stacked = jnp.concatenate([grow, left], axis=0)
     coarse = stacked.astype(BF16).astype(F32)
     split = jnp.concatenate([coarse, stacked - coarse], axis=0).T.astype(BF16)
-    spread = (
-        lax.broadcasted_iota(jnp.int32, (4 * heads, 2 * width), 1) // channels
-        == lax.broadcasted_iota(jnp.int32, (4 * heads, 2 * width), 0) % (2 * heads)
-    ).astype(BF16)
+    row_from = lax.broadcasted_iota(jnp.int32, (2 * heads, 2 * width), 0) * channels
+    lane = lax.broadcasted_iota(jnp.int32, (2 * heads, 2 * width), 1)
+    chosen = jnp.logical_and(lane >= row_from, lane < row_from + channels)
+    chosen = jnp.where(chosen, 1.0, 0.0).astype(BF16)
+    spread = jnp.concatenate([chosen, chosen], axis=0)
     wide = mm(split, spread)
     grow_wide, left_wide = wide[:, :width], wide[:, width:]
     last_wide = grow_wide[length - 1 : length]
 
-    @pl.when(first)
-    def _():
-        for ref in (head_halo, write_halo, read_halo, inner_halo, value_halo):
-            ref[...] = jnp.zeros_like(ref)
-
-    @pl.when(jnp.logical_not(first))
-    def _():
-        for copy in halos:
-            copy.wait_recv()
-
-    def causal_filter(pad, stream, before, taps):
+    def taps_over(pad, taps, rows, lanes):
         span = taps.shape[0]
-        pad[0:HALO, :] = before
-        pad[HALO : HALO + length, :] = stream
         total = None
         for k in range(span):
             start = HALO - (span - 1) + k
-            term = pad[start : start + length, :] * taps[k : k + 1]
+            term = pad[start : start + rows, lanes] * taps[k : k + 1, lanes].astype(F32)
             total = term if total is None else total + term
         return total
 
-    writes = silu(
-        causal_filter(
-            group_pad, writes_ref[0].astype(F32), write_halo[...].astype(F32), write_taps[...].astype(F32)
-        )
-    )
-    filtered = silu(
-        causal_filter(
-            head_pad, head_ref[0].astype(F32), head_halo[...].astype(F32), head_taps[...].astype(F32)
-        )
-    )
-    writes_t = [
-        writes[:, g * STATE : (g + 1) * STATE].T.astype(BF16) for g in range(groups)
-    ]
-    weighted = (filtered * left_wide).astype(BF16)
+    def fill(pad, stream):
+        pad[0:HALO, :] = jnp.zeros((HALO, pad.shape[1]), F32)
+        pad[HALO : HALO + length, :] = stream
+
+    every = slice(None)
+    fill(write_pad, writes_ref[0].astype(F32))
+    fill(head_pad, head_ref[0].astype(F32))
+    fill(read_pad, reads_ref[0].astype(F32))
+    fill(conv_pad, inner_ref[0].astype(F32) * value_ref[0].astype(F32))
+    write_act[...] = silu(taps_over(write_pad, write_taps, length, every))
     for g in range(groups):
-        piece = mm(writes_t[g], weighted[:, g * gw : (g + 1) * gw])
-        for i in range(per_group):
-            local_state[g * per_group + i] = piece[:, i * LANES : (i + 1) * LANES]
-
+        span = slice(g * gw, (g + 1) * gw)
+        head_act[:, span] = silu(taps_over(head_pad, head_taps, length, span))
+
+    @pl.when(jnp.logical_not(first))
+    def _():
+        for copy in halos:
+            copy.wait_recv()
+        for pad, halo in ((write_pad, write_halo), (head_pad, head_halo), (read_pad, read_halo)):
+            pad[0:HALO, :] = halo[...].astype(F32)
+        conv_pad[0:HALO, :] = inner_halo[...].astype(F32) * value_halo[...].astype(F32)
+        write_act[0:HALO, :] = silu(taps_over(write_pad, write_taps, HALO, every))
+        head_act[0:HALO, :] = silu(taps_over(head_pad, head_taps, HALO, every))
+
+    hstate = STATE // 2
     chain = [
-        remote(state_send.at[i], state_recv.at[i], state_ss.at[i], state_rs.at[i], nxt)
+        [
+            remote(state_send.at[i, h], state_recv.at[i, h], state_ss.at[i, h], state_rs.at[i, h], nxt)
+            for h in range(2)
+        ]
         for i in range(chunks)
     ]
-
-    @pl.when(first)
-    def _():
-        for i in range(chunks):
-            state_send[i] = local_state[i].astype(BF16)
-        for copy in chain:
-            copy.start()
-
-    product = inner_ref[0].astype(F32) * value_ref[0].astype(F32)
-    before = inner_halo[...].astype(F32) * value_halo[...].astype(F32)
-    convolved = causal_filter(conv_pad, product, before, conv_taps[...].astype(F32))
+    writes_t = []
+    for g in range(groups):
+        span = slice(g * gw, (g + 1) * gw)
+        writes_t.append(write_act[:, g * STATE : (g + 1) * STATE].T.astype(BF16))
+        weighted = (head_act[:, span] * left_wide[:, span]).astype(BF16)
+        piece = mm(writes_t[g], weighted)
+        for i in range(per_group):
+            k = g * per_group + i
+            part_of = piece[:, i * LANES : (i + 1) * LANES]
+            for h in range(2):
+                local_state[k, h] = part_of[h * hstate : (h + 1) * hstate]
+
+        @pl.when(first)
+        def _():
+            for i in range(g * per_group, (g + 1) * per_group):
+                state_send[i] = local_state[i].astype(BF16)
+            for i in range(g * per_group, (g + 1) * per_group):
+                for copy in chain[i]:
+                    copy.start()
+
+    convolved = taps_over(conv_pad, conv_taps, length, every)
     conv_rows = (outer_ref[0].astype(F32) * convolved).astype(BF16)
     conv_send[...] = conv_rows
     conv_copies = []
@@ -310,25 +309,37 @@
     def _():
         conv_home.start()
 
-    reads = silu(
-        causal_filter(
-            group_pad, reads_ref[0].astype(F32), read_halo[...].astype(F32), read_taps[...].astype(F32)
-        )
-    ).astype(BF16)
-    filtered16 = filtered.astype(BF16)
+    weights = []
+    for b in range(1, ntp):
+        other = at(sp, fs, lax.rem(tp + b, ntp))
+        weights.append(
+            remote(wconv_hbm, wconv.at[tp], weight_ss.at[b - 1, 0], weight_rs.at[b - 1, 0], other)
+        )
+        weights.append(
+            remote(wstate_hbm, wstate.at[tp], weight_ss.at[b - 1, 1], weight_rs.at[b - 1, 1], other)
+        )
+    for copy in weights:
+        copy.start()
+
+    reads = silu(taps_over(read_pad, read_taps, length, every)).astype(BF16)
     lane_head = lax.broadcasted_iota(jnp.int32, (length, LANES), 1) // channels
-    for g in range(groups):
-        scores = jnp.where(causal, mm(reads[:, g * STATE : (g + 1) * STATE], writes_t[g]), 0.0)
-        for i in range(g * per_group, (g + 1) * per_group):
-            block = filtered16[:, i * LANES : (i + 1) * LANES]
-            total = None
-            for r in range(hpl):
-                h = i * hpl + r
-                gaps = jnp.minimum(rising[:, h : h + 1] - rising_t[h : h + 1, :], 0.0)
-                mixed = (scores * jnp.exp(gaps) * dt_t[h : h + 1, :]).astype(BF16)
-                one = mm(mixed, block)
-                total = one if total is None else jnp.where(lane_head == r, one, total)
-            inside[:, i * LANES : (i + 1) * LANES] = total
+    scores = [
+        jnp.where(causal, mm(reads[:, g * STATE : (g + 1) * STATE], writes_t[g]), 0.0)
+        for g in range(groups)
+    ]
+
+    def within(i):
+        block = head_act[:, i * LANES : (i + 1) * LANES].astype(BF16)
+        total = None
+        for r in range(hpl):
+            h = i * hpl + r
+            gaps = jnp.minimum(rising[:, h : h + 1] - rising_t[h : h + 1, :], 0.0)
+            mixed = (scores[i // per_group] * jnp.exp(gaps) * dt_t[h : h + 1, :]).astype(BF16)
+            one = mm(mixed, block)
+            total = one if total is None else jnp.where(lane_head == r, one, total)
+        inside[:, i * LANES : (i + 1) * LANES] = total
+
+    within(0)
 
     home = dest == tp
     xfs = fs + 1 - 2 * lax.rem(fs, 2)
@@ -361,16 +372,17 @@
 
             @pl.when(jnp.logical_not(first))
             def _():
-                chain[i].wait_recv()
-                incoming = state_recv[i]
-
-                @pl.when(jnp.logical_not(last))
-                def _():
-                    state_send[i] = (
-                        incoming.astype(F32) * last_wide[:, lanes] + local_state[i]
-                    ).astype(BF16)
-                    chain[i].start()
-
+                for h in range(2):
+                    chain[i][h].wait_recv()
+
+                    @pl.when(jnp.logical_not(last))
+                    def _():
+                        state_send[i, h] = (
+                            state_recv[i, h].astype(F32) * last_wide[:, lanes] + local_state[i, h]
+                        ).astype(BF16)
+                        chain[i][h].start()
+
+                incoming = state_recv[i].reshape(STATE, LANES)
                 inside[:, lanes] += (
                     mm(reads[:, g * STATE : (g + 1) * STATE], incoming) * grow_wide[:, lanes]
                 )
@@ -392,6 +404,9 @@
                 @pl.when(jnp.logical_not(home))
                 def _():
                     branch_copy(u, 0, fs).start()
+
+            if i + 1 < chunks:
+                within(i + 1)
 
         factor = lax.rsqrt(jnp.sum(power, axis=1, keepdims=True) / gw + EPS)
         factor = jnp.broadcast_to(factor, (length, LANES)).T[:8]
@@ -512,8 +527,9 @@
     def _():
         for copy in halos:
             copy.wait_send()
-        for copy in chain:
-            copy.wait_send()
+        for pair in chain:
+            for copy in pair:
+                copy.wait_send()
 
     for copy in weights:
         copy.wait_send()
@@ -595,10 +611,13 @@
             pltpu.VMEM((HALO, conv_width), BF16),
             pltpu.VMEM((HALO + length, width), F32),
             pltpu.VMEM((HALO + length, group_width), F32),
+            pltpu.VMEM((HALO + length, group_width), F32),
+            pltpu.VMEM((length, width), F32),
+            pltpu.VMEM((length, group_width), F32),
             pltpu.VMEM((HALO + length, conv_width), F32),
-            pltpu.VMEM((chunks, STATE, LANES), F32),
-            pltpu.VMEM((chunks, STATE, LANES), BF16),
-            pltpu.VMEM((chunks, STATE, LANES), BF16),
+            pltpu.VMEM((chunks, 2, STATE // 2, LANES), F32),
+            pltpu.VMEM((chunks, 2, STATE // 2, LANES), BF16),
+            pltpu.VMEM((chunks, 2, STATE // 2, LANES), BF16),
             pltpu.VMEM((units, 2, half, width // units), BF16),
             pltpu.VMEM((per_tp, ntp, units, 2, half, width // units), BF16),
             pltpu.VMEM((groups, 8, length), F32),
@@ -613,8 +632,8 @@
             dma((7,)),
             dma((5,)),
             dma((5,)),
-            dma((chunks,)),
-            dma((chunks,)),
+            dma((chunks, 2)),
+            dma((chunks, 2)),
             dma((units, 3)),
             dma((per_tp, ntp, units)),
             dma((ntp, units)),

time: 28.2 us -> 28 us (level)
  no operation moved by 1% of the time
where the time goes in v3:
time: 28 us; the launch traced here: 27.7 us
  Pallas kernels  26 us (93%)
  local copies, waits for them, and re-layouts  1.67 us (6%)
    pallas_call x1, Pallas kernels, per_device(): pl.pallas_call(functools.partial(kernel, sizes), out_shape=jax.ShapeDtype...  26 us
    unnamed x1, local copies, waits for them, and re-layouts  1.67 us

profile of v3, /device:TPU:25, one launch (start us, length us, event | category | flops | bytes accessed | tf_op | source)
XLA Modules:
  0.0 27.7 jit_solution(17020012851969429543)
XLA Ops:
  0.0 26.0 %shard_map.172 = bf16[2,128,512]{2,1,0:T(8,128)(2,1)} custom-call(bf16[1,128,1024]{2,1,0:T(8,128)(2,1)} %gate_hbm.1, bf16[1,128,1024]{2,1,0:T(8,128)(2,1)} %head_hbm.1, bf16[1,128,256]{2,1,0:T(8,128)(2,1)} %writes_hbm.1, bf16[1,128,256]{2,1,0:T(8,128)(2,1)} %reads_hbm.1, f32[1,16,128]{2,1,0:T(8,128)} %bitcast.5, f32[1,16]{1,0:T(1,128)} %bitcast.8, ...), custom_call_target="tpu_custom_call" | custom-call | tf_op jit(solution)/shard_map/pallas_call | solution.py:594
  26.0 1.7 %copy.20 = bf16[2,128,512]{2,1,0:T(8,128)(2,1)} copy(bf16[2,128,512]{2,1,0:T(8,128)(2,1)} %shard_map.172) | data formatting | bytes 524288
